TPU v7x, 32 devices: a whole 2x2x4 slice. The times are simulated.
32 devices in a mesh: dp: 4 (over y, x), kv: 4 (over z), tp: 2 (over core).
Axes of the slice: x: 2, y: 2, z: 4, core: 2. Of those that a mesh axis runs over, the one named last changes fastest.
Arguments:
- resid: bfloat16 [16, 2048], P('dp', ('kv', 'tp')), may hold values from -45 to 45
- norm_gain: bfloat16 [3, 2048], P(None, ('kv', 'tp')), may hold values from 0.099609375 to 1.8984375
- ffn_gate: bfloat16 [2, 2048, 5632], P(None, None, ('kv', 'tp')), may hold values from -0.125 to 0.125
- ffn_up: bfloat16 [2, 2048, 5632], P(None, None, ('kv', 'tp')), may hold values from -0.125 to 0.125
- ffn_down: bfloat16 [2, 5632, 2048], P(None, ('kv', 'tp')), may hold values from -0.109375 to 0.109375
- w_x: bfloat16 [2048, 64, 64], P(None, 'kv', 'tp'), may hold values from -0.125 to 0.125
- w_z: bfloat16 [2048, 64, 64], P(None, 'kv', 'tp'), may hold values from -0.125 to 0.125
- w_bc: bfloat16 [2048, 2, 8, 128], P('kv'), may hold values from -0.125 to 0.125
- w_dt: bfloat16 [2048, 64], P('kv'), may hold values from -0.125 to 0.125
- dt_bias: float32 [64], replicated, may hold values from -2 to 0.5
- a_log: float32 [64], replicated, may hold values from -1.5 to 1.5
- d_skip: float32 [64], replicated, may hold values from 0.5 to 1.5
- conv_wx: bfloat16 [4, 64, 64], P(None, None, 'tp'), may hold values from -3 to 3
- conv_wbc: bfloat16 [4, 2, 8, 128], replicated, may hold values from -3 to 3
- conv_x: bfloat16 [16, 3, 64, 64], P(('dp', 'kv'), None, None, 'tp'), may hold values from -6 to 6
- conv_bc: bfloat16 [16, 3, 2, 8, 128], P(('dp', 'kv')), may hold values from -6 to 6
- ssm_state: float32 [16, 64, 64, 128], P(('dp', 'kv'), None, 'tp'), may hold values from -3 to 3
- w_out: bfloat16 [64, 64, 2048], P(None, 'tp', 'kv'), may hold values from -0.09375 to 0.09375
Outputs:
- final: bfloat16 [16, 2048], P('dp', ('kv', 'tp'))
All inputs are finite; a program needn't handle non-finite values.
Results may differ from a plain program's by a relative error of at most 0.018.
Values may be sent and summed in bfloat16 or wider, within the bound.
No kernel may reach another device: no remote copies, remote signals or barrier semaphores. Data moves between devices by JAX's collectives and lax.ppermute only.
A program may use at most 64 MiB of HBM per device.

v0:
```python
import jax
import jax.numpy as jnp
from jax import lax
from jax.sharding import PartitionSpec as P

D = 2048
EPS = 1e-06


def normalize(rows, gain):
    values = rows.astype(jnp.float32)
    scale = lax.rsqrt(jnp.mean(values * values, axis=1, keepdims=True) + EPS)
    return (values * scale * gain.astype(jnp.float32).reshape(1, -1)).astype(jnp.bfloat16)


def feed_forward(normed, w_gate, w_up, w_down):
    gate = jnp.dot(normed, w_gate, preferred_element_type=jnp.float32)
    upper = jnp.dot(normed, w_up, preferred_element_type=jnp.float32)
    hidden = (jax.nn.silu(gate) * upper).astype(jnp.bfloat16)
    return jnp.dot(hidden, w_down, preferred_element_type=jnp.float32)


def add_half(base, sums):
    return (base.astype(jnp.float32) + 0.5 * sums).astype(jnp.bfloat16)


def ffn_totals(partial_value):
    return lax.psum(partial_value, ("kv", "tp"))


def short_conv(history, newest, taps):
    window = jnp.concatenate(
        [history.astype(jnp.float32), newest.astype(jnp.float32)[:, None]], axis=1
    )
    return jax.nn.silu(jnp.sum(window * taps.astype(jnp.float32)[None], axis=1))


def state_step(
    xs_new,
    zeta,
    bc_new,
    dt_raw,
    conv_x,
    conv_bc,
    ssm_state,
    conv_wx,
    conv_wbc,
    dt_bias,
    a_log,
    d_skip,
):
    xconv = short_conv(conv_x, xs_new, conv_wx)
    bconv = short_conv(conv_bc, bc_new, conv_wbc)
    heads = xconv.shape[1]
    groups = bconv.shape[2]
    bmat = jnp.repeat(bconv[:, 0], heads // groups, axis=1)
    cmat = jnp.repeat(bconv[:, 1], heads // groups, axis=1)
    step_size = jax.nn.softplus(dt_raw + dt_bias[None, :])
    decay = jnp.exp(-step_size * jnp.exp(a_log)[None, :])
    updated = (
        decay[:, :, None, None] * ssm_state
        + (step_size[:, :, None] * xconv)[..., None] * bmat[:, :, None, :]
    )
    mixed = (
        jnp.einsum("shpn,shn->shp", updated, cmat, precision=lax.Precision.HIGHEST)
        + d_skip[None, :, None] * xconv
    )
    return (mixed * jax.nn.silu(zeta.astype(jnp.float32))).astype(jnp.bfloat16)


def group_terms(slab, w_bc, w_dt):
    span = slab.shape[1]
    flat_bc = w_bc.reshape(span, -1)
    bc_part = jnp.dot(slab, flat_bc, preferred_element_type=jnp.float32)
    dt_part = jnp.dot(slab, w_dt, preferred_element_type=jnp.float32)
    return (
        lax.psum_scatter(bc_part, "kv", scatter_dimension=0, tiled=True),
        lax.psum_scatter(dt_part, "kv", scatter_dimension=0, tiled=True),
    )


def mix_partial(
    normed,
    w_x,
    w_z,
    w_bc,
    w_dt,
    dt_bias,
    a_log,
    d_skip,
    conv_wx,
    conv_wbc,
    conv_x,
    conv_bc,
    ssm_state,
    w_out,
):
    rows = normed.shape[0]
    local_heads = w_x.shape[1]
    half = w_x.shape[2]
    xs_part = (
        jnp.dot(normed, w_x.reshape(D, -1), preferred_element_type=jnp.float32)
        .astype(jnp.bfloat16)
        .reshape(rows, local_heads, half)
    )
    zeta_part = (
        jnp.dot(normed, w_z.reshape(D, -1), preferred_element_type=jnp.float32)
        .astype(jnp.bfloat16)
        .reshape(rows, local_heads, half)
    )
    xs_new, zeta = (
        lax.all_to_all(xs_part, "kv", split_axis=0, concat_axis=1, tiled=True),
        lax.all_to_all(zeta_part, "kv", split_axis=0, concat_axis=1, tiled=True),
    )
    span = w_bc.shape[0]
    slab = lax.dynamic_slice_in_dim(normed, lax.axis_index("kv") * span, span, 1)
    bc_sum, dt_raw = group_terms(slab, w_bc, w_dt)
    bc_new = bc_sum.astype(jnp.bfloat16).reshape((bc_sum.shape[0],) + w_bc.shape[1:])
    mixed = state_step(
        xs_new,
        zeta,
        bc_new,
        dt_raw,
        conv_x,
        conv_bc,
        ssm_state,
        conv_wx,
        conv_wbc,
        dt_bias,
        a_log,
        d_skip,
    )
    flat_out = w_out.reshape(-1, w_out.shape[2])
    piece = lax.all_gather(mixed, "kv", axis=0, tiled=True)
    return jnp.dot(piece.reshape(piece.shape[0], -1), flat_out, preferred_element_type=jnp.float32)


def per_device(
    resid,
    norm_gain,
    ffn_gate,
    ffn_up,
    ffn_down,
    w_x,
    w_z,
    w_bc,
    w_dt,
    dt_bias,
    a_log,
    d_skip,
    conv_wx,
    conv_wbc,
    conv_x,
    conv_bc,
    ssm_state,
    w_out,
):
    mixer_args = (
        w_x,
        w_z,
        w_bc,
        w_dt,
        dt_bias,
        a_log,
        d_skip,
        conv_wx,
        conv_wbc,
        conv_x,
        conv_bc,
        ssm_state,
        w_out,
    )
    rows, gains = (
        lax.all_gather(resid, ("kv", "tp"), axis=1, tiled=True),
        lax.all_gather(norm_gain, ("kv", "tp"), axis=1, tiled=True),
    )
    first = add_half(
        rows,
        ffn_totals(feed_forward(normalize(rows, gains[0]), ffn_gate[0], ffn_up[0], ffn_down[0])),
    )
    partial_value = mix_partial(normalize(first, gains[1]), *mixer_args)
    span = partial_value.shape[1]
    block = lax.dynamic_slice_in_dim(first, lax.axis_index("kv") * span, span, 1)
    joined = (block.astype(jnp.float32) + lax.psum(partial_value, "tp")).astype(jnp.bfloat16)
    second = lax.all_gather(joined, "kv", axis=1, tiled=True)
    final = add_half(
        second,
        ffn_totals(feed_forward(normalize(second, gains[2]), ffn_gate[1], ffn_up[1], ffn_down[1])),
    )
    width = resid.shape[1]
    return lax.dynamic_slice_in_dim(final, lax.axis_index(("kv", "tp")) * width, width, 1)


def solution(mesh):
    placed = (
        P("dp", ("kv", "tp")),
        P(None, ("kv", "tp")),
        P(None, None, ("kv", "tp")),
        P(None, None, ("kv", "tp")),
        P(None, ("kv", "tp"), None),
        P(None, "kv", "tp"),
        P(None, "kv", "tp"),
        P("kv", None, None, None),
        P("kv", None),
        P(),
        P(),
        P(),
        P(None, None, "tp"),
        P(),
        P(("dp", "kv"), None, None, "tp"),
        P(("dp", "kv"), None, None, None, None),
        P(("dp", "kv"), None, "tp", None),
        P(None, "tp", "kv"),
    )
    return jax.shard_map(
        per_device, mesh=mesh, in_specs=placed, out_specs=P("dp", ("kv", "tp")), check_vma=False
    )
```

profile of v0, /device:TPU:0, one launch (start us, length us, event | category | flops | bytes accessed | tf_op | source)
XLA Modules:
  0.0 168.5 jit_solution(16530086735748407296)
XLA Ops:
  0.0 14.7 %all_gather.12 = bf16[4,2048]{1,0:T(4,128)(2,1)S(1)} all-gather(bf16[4,256]{1,0:T(4,128)(2,1)} %param.18), channel_id=1, replica_groups=mesh['dp'=4,'kv'=4,'tp'=2] {'kv','tp'}, dimensions={1}, use_global_device_ids=true | all-gather | bytes 18432 | tf_op jit(solution)/shard_map/all_gather | solution.py:174
  14.9 12.9 %all_gather.13 = bf16[3,2048]{1,0:T(4,128)(2,1)S(1)} all-gather(bf16[3,256]{1,0:T(4,128)(2,1)} %param.19), channel_id=1, replica_groups=mesh['dp'=4,'kv'=4,'tp'=2] {'kv','tp'}, dimensions={1}, use_global_device_ids=true | all-gather | bytes 13824 | tf_op jit(solution)/shard_map/all_gather | solution.py:175
  27.8 2.7 %fusion.10 = f32[4,704]{1,0:T(4,128)S(1)} fusion(bf16[2,2048,704]{1,2,0:T(8,128)(2,1)} %param.20, bf16[4,2048]{1,0:T(4,128)(2,1)S(1)} %all_gather.12, f32[2048]{0:T(1024)S(1)} %bitcast.113, f32[4]{0:T(128)S(1)} %add_rsqrt_fusion.2), kind=kOutput, calls=%fused_computation.10 | convolution fusion | flops 11567104 | bytes 2919440 | tf_op jit(solution)/shard_map/dot_general | solution.py:17
  30.5 4.4 %fusion.6 = f32[4,2048]{1,0:T(4,128)S(1)} fusion(bf16[2,704,2048]{2,1,0:T(8,128)(2,1)} %param.22, bf16[2,2048,704]{1,2,0:T(8,128)(2,1)} %param.21, f32[4,704]{1,0:T(4,128)S(1)} %fusion.10, bf16[4,2048]{1,0:T(4,128)(2,1)S(1)} %all_gather.12, f32[2048]{0:T(1024)S(1)} %bitcast.114, f32[4]{0:T(128)S(1)} %add_rsqrt_fusion.2), kind=kOutput, calls=%fused_computation.6 | convolution fusion | flops 23118336 | bytes 5835792 | tf_op jit(solution)/shard_map/dot_general | solution.py:20
  34.8 26.7 %psum.21 = f32[4,2048]{1,0:T(4,128)S(1)} all-reduce(f32[4,2048]{1,0:T(4,128)S(1)} %fusion.6), channel_id=1, replica_groups=mesh['dp'=4,'kv'=4,'tp'=2] {'kv','tp'}, use_global_device_ids=true, to_apply=%region_1.2 | all-reduce | flops 8192 | bytes 65536 | tf_op jit(solution)/shard_map/psum | solution.py:28
  61.8 0.6 convolution_convert_fusion.1
  62.5 0.7 reshape.219
  63.2 3.2 %all-to-all-start = ((bf16[4,2,256]{2,1,0:T(2,128)(2,1)}), bf16[4,2,256]{2,1,0:T(2,128)(2,1)S(1)}, u32[]{:S(2)}, u32[]{:S(2)}) async-start(bf16[4,2,256]{2,1,0:T(2,128)(2,1)} %reshape.219), calls=%async_computation | async-start | bytes 8192 | tf_op jit(solution)/shard_map/all_to_all | solution.py:112
  66.5 2.2 %convolution_convert_fusion = bf16[4,512]{1,0:T(4,128)(2,1)S(1)} fusion(bf16[4,2048]{1,0:T(4,128)(2,1)S(1)} %fusion.47, bf16[2048,512]{0,1:T(8,128)(2,1)} %bitcast.109), kind=kOutput, calls=%fused_computation.26 | convolution fusion | flops 8390656 | bytes 2117632 | tf_op jit(solution)/shard_map/dot_general | solution.py:107
  68.9 2.0 %fusion.18 = f32[4,2048]{1,0:T(4,128)S(1)} fusion(bf16[64,8,16,128]{3,2,1,0:T(8,128)(2,1)} %bitcast.108, bf16[4,2048]{1,0:T(4,128)(2,1)S(1)} %fusion.47, s32[]{:T(128)S(6)} %select_n.11), kind=kOutput, calls=%fused_computation.18 | convolution fusion | flops 8388608 | bytes 2134020 | tf_op jit(solution)/shard_map/dot_general | solution.py:74
  71.4 19.8 %all-reduce.2 = (bf16[4,2048]{1,0:T(4,128)(2,1)S(1)}, f32[4,64]{1,0:T(4,128)S(1)}) all-reduce(f32[4,2048]{1,0:T(4,128)S(1)} %fusion.18, f32[4,64]{1,0:T(4,128)S(1)} %fusion.69), channel_id=4, replica_groups=mesh['dp'=4,'kv'=4,'tp'=2] {'kv'}, use_global_device_ids=true, to_apply=%region_5.6.clone | all-reduce | flops 8448 | bytes 51200
  91.2 0.7 fusion.60
  92.1 0.7 reshape.217
  92.8 3.2 %all-to-all-start.1 = ((bf16[4,2,256]{2,1,0:T(2,128)(2,1)}), bf16[4,2,256]{2,1,0:T(2,128)(2,1)S(1)}, u32[]{:S(2)}, u32[]{:S(2)}) async-start(bf16[4,2,256]{2,1,0:T(2,128)(2,1)} %reshape.217), calls=%async_computation.1 | async-start | bytes 8192 | tf_op jit(solution)/shard_map/all_to_all | solution.py:113
  96.0 0.7 fusion.75
  96.9 4.7 %all-to-all-done.1 = bf16[4,2,256]{2,1,0:T(2,128)(2,1)S(1)} async-done(((bf16[4,2,256]{2,1,0:T(2,128)(2,1)}), bf16[4,2,256]{2,1,0:T(2,128)(2,1)S(1)}, u32[]{:S(2)}, u32[]{:S(2)}) %all-to-all-start.1) | async-done | bytes 4128 | tf_op jit(solution)/shard_map/all_to_all | solution.py:113
  101.9 1.9 %fusion.33 = f32[64,1,32]{2,1,0:T(1,128)S(1)} fusion(f32[64,128,1]{1,2,0:T(1,128)S(1)} %bitcast.110, f32[1,64,32,128]{3,2,1,0:T(8,128)S(1)} %copy-done.1, f32[64,128]{1,0:T(8,128)S(1)} %broadcast_bitcast_fusion, f32[64,32]{1,0:T(8,128)S(1)} %copy.28, f32[64]{0:T(128)S(1)} %get-tuple-element.7), kind=kOutput, calls=%fused_computation.28 | convolution fusion | flops 3932160 | bytes 1130752 | tf_op jit(solution)/shard_map/shpn,shn->shp/dot_general | solution.py:65
  103.9 13.1 %all-gather.1 = bf16[4,64,32]{1,2,0:T(8,128)(2,1)S(1)} all-gather(bf16[1,64,32]{1,2,0:T(8,128)(2,1)S(1)} %fusion.64), channel_id=2, replica_groups=mesh['dp'=4,'kv'=4,'tp'=2] {'kv'}, dimensions={0}, use_global_device_ids=true | all-gather | bytes 20480 | tf_op jit(solution)/shard_map/all_gather | solution.py:134
  117.1 2.0 %convolution_bitcast_fusion = f32[4,512]{1,0:T(4,128)S(1)} fusion(bf16[4,64,32]{2,0,1:T(4,128)(2,1)S(1)} %copy.35, bf16[64,32,512]{2,1,0:T(8,128)(2,1)} %param.35), kind=kOutput, calls=%fused_computation.25 | convolution fusion | flops 8388608 | bytes 2121728 | tf_op jit(solution)/shard_map/dot_general | solution.py:135
  119.2 2.5 %psum.22 = f32[4,512]{1,0:T(4,128)S(1)} all-reduce(f32[4,512]{1,0:T(4,128)S(1)} %convolution_bitcast_fusion), channel_id=1, replica_groups=mesh['dp'=4,'kv'=4,'tp'=2] {'tp'}, use_global_device_ids=true, to_apply=%region_7.8 | all-reduce | flops 2048 | bytes 16384 | tf_op jit(solution)/shard_map/psum | solution.py:184
  121.6 13.2 %all_gather.15 = bf16[4,2048]{1,0:T(4,128)(2,1)S(1)} all-gather(bf16[4,512]{1,0:T(4,128)(2,1)S(1)} %add_convert_fusion), channel_id=1, replica_groups=mesh['dp'=4,'kv'=4,'tp'=2] {'kv'}, dimensions={1}, use_global_device_ids=true | all-gather | bytes 20480 | tf_op jit(solution)/shard_map/all_gather | solution.py:185
  135.0 2.7 %fusion.4 = f32[4,704]{1,0:T(4,128)S(1)} fusion(bf16[2,2048,704]{1,2,0:T(8,128)(2,1)} %param.20, f32[2048]{0:T(1024)S(1)} %bitcast.111, f32[4]{0:T(128)S(1)} %add_rsqrt_fusion, bf16[4,2048]{1,0:T(4,128)(2,1)S(1)} %all_gather.15), kind=kOutput, calls=%fused_computation.4 | convolution fusion | flops 11567104 | bytes 2919440 | tf_op jit(solution)/shard_map/dot_general | solution.py:17
  137.7 4.4 %fusion = f32[4,2048]{1,0:T(4,128)S(1)} fusion(bf16[2,704,2048]{2,1,0:T(8,128)(2,1)} %param.22, bf16[2,2048,704]{1,2,0:T(8,128)(2,1)} %param.21, f32[4,704]{1,0:T(4,128)S(1)} %fusion.4, f32[2048]{0:T(1024)S(1)} %bitcast.112, f32[4]{0:T(128)S(1)} %add_rsqrt_fusion, bf16[4,2048]{1,0:T(4,128)(2,1)S(1)} %all_gather.15), kind=kOutput, calls=%fused_computation | convolution fusion | flops 23118336 | bytes 5835792 | tf_op jit(solution)/shard_map/dot_general | solution.py:20
  142.0 25.9 %psum.23 = f32[4,2048]{1,0:T(4,128)S(1)} all-reduce(f32[4,2048]{1,0:T(4,128)S(1)} %fusion), channel_id=1, replica_groups=mesh['dp'=4,'kv'=4,'tp'=2] {'kv','tp'}, use_global_device_ids=true, to_apply=%region_9.10 | all-reduce | flops 8192 | bytes 65536 | tf_op jit(solution)/shard_map/psum | solution.py:28
  (54 shorter events, 2.8 us)
Async XLA Ops:
  0.0 61.7 %copy-start = (bf16[2048,16,32]{0,2,1:T(8,128)(2,1)S(1)}, bf16[2048,16,32]{0,2,1:T(8,128)(2,1)}, u32[]{:S(2)}) copy-start(bf16[2048,16,32]{0,2,1:T(8,128)(2,1)} %param.23) | copy-start | bytes 6291460
  34.8 33.9 %copy-start.2 = (bf16[512,64]{0,1:T(8,128)(2,1)S(1)}, bf16[512,64]{0,1:T(8,128)(2,1)}, u32[]{:S(2)}) copy-start(bf16[512,64]{0,1:T(8,128)(2,1)} %param.26) | copy-start | bytes 196612
  61.7 9.1 %copy-start.10 = (u32[32]{0:T(128)S(1)}, u32[32]{0:T(128)}, u32[]{:S(2)}) copy-start(u32[32]{0:T(128)} %constant.45) | copy-start | bytes 388
  61.7 30.2 %copy-start.5 = (bf16[4,2,8,128]{3,2,1,0:T(8,128)(2,1)S(1)}, bf16[4,2,8,128]{3,2,1,0:T(8,128)(2,1)}, u32[]{:S(2)}) copy-start(bf16[4,2,8,128]{3,2,1,0:T(8,128)(2,1)} %param.31) | copy-start | bytes 49156
  61.8 30.2 %copy-start.6 = (bf16[1,3,2,8,128]{4,3,2,1,0:T(8,128)(2,1)S(1)}, bf16[1,3,2,8,128]{4,3,2,1,0:T(8,128)(2,1)}, u32[]{:S(2)}) copy-start(bf16[1,3,2,8,128]{4,3,2,1,0:T(8,128)(2,1)} %param.33) | copy-start | bytes 36868
  61.8 34.2 %copy-start.8 = (f32[64]{0:T(128)S(1)}, f32[64]{0:T(128)}, u32[]{:S(2)}) copy-start(f32[64]{0:T(128)} %param.28) | copy-start | bytes 772
  61.8 34.2 %copy-start.9 = (f32[64]{0:T(128)S(1)}, f32[64]{0:T(128)}, u32[]{:S(2)}) copy-start(f32[64]{0:T(128)} %param.27) | copy-start | bytes 772
  62.4 39.3 %copy-start.3 = (bf16[4,64,32]{1,2,0:T(8,128)(2,1)S(1)}, bf16[4,64,32]{1,2,0:T(8,128)(2,1)}, u32[]{:S(2)}) copy-start(bf16[4,64,32]{1,2,0:T(8,128)(2,1)} %param.30) | copy-start | bytes 49156
  62.4 39.3 %copy-start.4 = (bf16[1,3,64,32]{2,3,1,0:T(8,128)(2,1)S(1)}, bf16[1,3,64,32]{2,3,1,0:T(8,128)(2,1)}, u32[]{:S(2)}) copy-start(bf16[1,3,64,32]{2,3,1,0:T(8,128)(2,1)} %param.32) | copy-start | bytes 36868
  62.4 39.4 %copy-start.1 = (f32[1,64,32,128]{3,2,1,0:T(8,128)S(1)}, f32[1,64,32,128]{3,2,1,0:T(8,128)}, u32[]{:S(2)}) copy-start(f32[1,64,32,128]{3,2,1,0:T(8,128)} %param.34) | copy-start | bytes 3145732
  63.2 29.5 %all-to-all-start = ((bf16[4,2,256]{2,1,0:T(2,128)(2,1)}), bf16[4,2,256]{2,1,0:T(2,128)(2,1)S(1)}, u32[]{:S(2)}, u32[]{:S(2)}) async-start(bf16[4,2,256]{2,1,0:T(2,128)(2,1)} %reshape.219), calls=%async_computation | async-start | bytes 8192 | tf_op jit(solution)/shard_map/all_to_all | solution.py:112
  66.5 37.4 %copy-start.7 = (f32[64]{0:T(128)S(1)}, f32[64]{0:T(128)}, u32[]{:S(2)}) copy-start(f32[64]{0:T(128)} %param.29) | copy-start | bytes 772
  92.8 8.8 %all-to-all-start.1 = ((bf16[4,2,256]{2,1,0:T(2,128)(2,1)}), bf16[4,2,256]{2,1,0:T(2,128)(2,1)S(1)}, u32[]{:S(2)}, u32[]{:S(2)}) async-start(bf16[4,2,256]{2,1,0:T(2,128)(2,1)} %reshape.217), calls=%async_computation.1 | async-start | bytes 8192 | tf_op jit(solution)/shard_map/all_to_all | solution.py:113
where the time goes:
time: 169 us
  blocking collectives  129 us (76%)
  matrix products  22.9 us (14%)
  starting transfers between devices  6.47 us (4%)
  waiting for transfers between devices  4.68 us (3%)
  local copies, waits for them, and re-layouts  3.47 us (2%)
  other arithmetic  1.89 us (1%)
    psum x2, blocking collectives, ffn_totals(): return lax.psum(partial_value, ('kv', 'tp'))  52.6 us
    unnamed x1, blocking collectives  19.8 us
    all_gather x1, blocking collectives, per_device(): lax.all_gather(resid, ('kv', 'tp'), axis=1, tiled=True)  14.7 us
    all_gather x1, blocking collectives, per_device(): second = lax.all_gather(joined, 'kv', axis=1, tiled=True)  13.2 us
    all_gather x1, blocking collectives, mix_partial(): piece = lax.all_gather(mixed, 'kv', axis=0, tiled=True)  13.1 us
    all_gather x1, blocking collectives, per_device(): lax.all_gather(norm_gain, ('kv', 'tp'), axis=1, tiled=True)  12.9 us
    dot_general x2, matrix products, feed_forward(): return jnp.dot(hidden, w_down, preferred_element_type=jnp.float32)  8.72 us
    dot_general x2, matrix products, feed_forward(): gate = jnp.dot(normed, w_gate, preferred_element_type=jnp.float32)  5.31 us
  transfers between devices with their start and end apart: 2, of which 1 were waited for; matrix products, arithmetic and copies ran while one was open for 4% of the time, Pallas kernels for 0%

commit v1 on v0

--- a/solution.py
+++ b/solution.py
@@ -2,6 +2,7 @@
 import jax.numpy as jnp
 from jax import lax
 from jax.sharding import PartitionSpec as P
+from jax.lax import psum
 
 D = 2048
 EPS = 1e-06
@@ -25,7 +26,8 @@
 
 
 def ffn_totals(partial_value):
-    return lax.psum(partial_value, ("kv", "tp"))
+    kinds_measure = lambda load, link_axis, mesh_ax: psum(psum(load, axis_name=link_axis), mesh_ax)
+    return kinds_measure(partial_value, "kv", "tp")
 
 
 def short_conv(history, newest, taps):

time: 169 us -> 156 us (0.923)
  blocking collectives: 129 us -> 116 us
    psum x2 -> x4, blocking collectives: 52.6 us -> 39.6 us  [the longest x2 32.8 us: ffn_totals(): psum(load, axis_name=link_axis)]
  transfers between devices with their start and end apart: 2 -> 2, of which waited for: 1 -> 1; matrix products, arithmetic and copies ran while one was open for 4% -> 5% of each run, Pallas kernels for 0% -> 0%
where the time goes in v1:
time: 156 us
  blocking collectives  116 us (74%)
  matrix products  22.9 us (15%)
  starting transfers between devices  6.47 us (4%)
  waiting for transfers between devices  4.68 us (3%)
  local copies, waits for them, and re-layouts  3.47 us (2%)
  other arithmetic  1.9 us (1%)
    psum x2, blocking collectives, ffn_totals(): psum(load, axis_name=link_axis)  32.8 us
    unnamed x1, blocking collectives  19.8 us
    all_gather x1, blocking collectives, per_device(): lax.all_gather(resid, ('kv', 'tp'), axis=1, tiled=True)  14.7 us
    all_gather x1, blocking collectives, per_device(): second = lax.all_gather(joined, 'kv', axis=1, tiled=True)  13.2 us
    all_gather x1, blocking collectives, mix_partial(): piece = lax.all_gather(mixed, 'kv', axis=0, tiled=True)  13.1 us
    all_gather x1, blocking collectives, per_device(): lax.all_gather(norm_gain, ('kv', 'tp'), axis=1, tiled=True)  12.9 us
    dot_general x2, matrix products, feed_forward(): return jnp.dot(hidden, w_down, preferred_element_type=jnp.float32)  8.72 us
    psum x2, blocking collectives, ffn_totals(): psum(psum(load, axis_name=link_axis), mesh_ax)  6.81 us
  transfers between devices with their start and end apart: 2, of which 1 were waited for; matrix products, arithmetic and copies ran while one was open for 5% of the time, Pallas kernels for 0%

profile of v1, /device:TPU:0, one launch (start us, length us, event | category | flops | bytes accessed | tf_op | source)
XLA Modules:
  0.0 155.6 jit_solution(6570567856445073053)
XLA Ops:
  0.0 14.7 %all_gather.12 = bf16[4,2048]{1,0:T(4,128)(2,1)S(1)} all-gather(bf16[4,256]{1,0:T(4,128)(2,1)} %param.18), channel_id=1, replica_groups=mesh['dp'=4,'kv'=4,'tp'=2] {'kv','tp'}, dimensions={1}, use_global_device_ids=true | all-gather | bytes 18432 | tf_op jit(solution)/shard_map/all_gather | solution.py:176
  14.9 12.9 %all_gather.13 = bf16[3,2048]{1,0:T(4,128)(2,1)S(1)} all-gather(bf16[3,256]{1,0:T(4,128)(2,1)} %param.19), channel_id=1, replica_groups=mesh['dp'=4,'kv'=4,'tp'=2] {'kv','tp'}, dimensions={1}, use_global_device_ids=true | all-gather | bytes 13824 | tf_op jit(solution)/shard_map/all_gather | solution.py:177
  27.8 2.7 %fusion.10 = f32[4,704]{1,0:T(4,128)S(1)} fusion(bf16[2,2048,704]{1,2,0:T(8,128)(2,1)} %param.20, bf16[4,2048]{1,0:T(4,128)(2,1)S(1)} %all_gather.12, f32[2048]{0:T(1024)S(1)} %bitcast.113, f32[4]{0:T(128)S(1)} %add_rsqrt_fusion.2), kind=kOutput, calls=%fused_computation.10 | convolution fusion | flops 11567104 | bytes 2919440 | tf_op jit(solution)/shard_map/dot_general | solution.py:18
  30.5 4.4 %fusion.6 = f32[4,2048]{1,0:T(4,128)S(1)} fusion(bf16[2,704,2048]{2,1,0:T(8,128)(2,1)} %param.22, bf16[2,2048,704]{1,2,0:T(8,128)(2,1)} %param.21, f32[4,704]{1,0:T(4,128)S(1)} %fusion.10, bf16[4,2048]{1,0:T(4,128)(2,1)S(1)} %all_gather.12, f32[2048]{0:T(1024)S(1)} %bitcast.114, f32[4]{0:T(128)S(1)} %add_rsqrt_fusion.2), kind=kOutput, calls=%fused_computation.6 | convolution fusion | flops 23118336 | bytes 5835792 | tf_op jit(solution)/shard_map/dot_general | solution.py:21
  34.8 16.6 %psum.35 = f32[4,2048]{1,0:T(4,128)S(1)} all-reduce(f32[4,2048]{1,0:T(4,128)S(1)} %fusion.6), channel_id=1, replica_groups=mesh['dp'=4,'kv'=4,'tp'=2] {'kv'}, use_global_device_ids=true, to_apply=%region_1.2 | all-reduce | flops 8192 | bytes 65536 | tf_op jit(solution)/shard_map/psum | solution.py:29
  51.4 3.4 %psum.36 = f32[4,2048]{1,0:T(4,128)S(1)} all-reduce(f32[4,2048]{1,0:T(4,128)S(1)} %psum.35), channel_id=1, replica_groups=mesh['dp'=4,'kv'=4,'tp'=2] {'tp'}, use_global_device_ids=true, to_apply=%region_2.3 | all-reduce | flops 8192 | bytes 65536 | tf_op jit(solution)/shard_map/psum | solution.py:29
  55.9 0.7 reshape.219
  56.6 3.2 %all-to-all-start = ((bf16[4,2,256]{2,1,0:T(2,128)(2,1)}), bf16[4,2,256]{2,1,0:T(2,128)(2,1)S(1)}, u32[]{:S(2)}, u32[]{:S(2)}) async-start(bf16[4,2,256]{2,1,0:T(2,128)(2,1)} %reshape.219), calls=%async_computation | async-start | bytes 8192 | tf_op jit(solution)/shard_map/all_to_all | solution.py:114
  59.8 2.2 %convolution_convert_fusion = bf16[4,512]{1,0:T(4,128)(2,1)S(1)} fusion(bf16[4,2048]{1,0:T(4,128)(2,1)S(1)} %fusion.47, bf16[2048,512]{0,1:T(8,128)(2,1)} %bitcast.109), kind=kOutput, calls=%fused_computation.26 | convolution fusion | flops 8390656 | bytes 2117632 | tf_op jit(solution)/shard_map/dot_general | solution.py:109
  62.2 2.0 %fusion.18 = f32[4,2048]{1,0:T(4,128)S(1)} fusion(bf16[64,8,16,128]{3,2,1,0:T(8,128)(2,1)} %bitcast.108, bf16[4,2048]{1,0:T(4,128)(2,1)S(1)} %fusion.47, s32[]{:T(128)S(6)} %select_n.11), kind=kOutput, calls=%fused_computation.18 | convolution fusion | flops 8388608 | bytes 2134020 | tf_op jit(solution)/shard_map/dot_general | solution.py:76
  64.8 19.8 %all-reduce.2 = (bf16[4,2048]{1,0:T(4,128)(2,1)S(1)}, f32[4,64]{1,0:T(4,128)S(1)}) all-reduce(f32[4,2048]{1,0:T(4,128)S(1)} %fusion.18, f32[4,64]{1,0:T(4,128)S(1)} %fusion.69), channel_id=4, replica_groups=mesh['dp'=4,'kv'=4,'tp'=2] {'kv'}, use_global_device_ids=true, to_apply=%region_6.7.clone | all-reduce | flops 8448 | bytes 51200
  84.6 0.7 fusion.60
  85.4 0.7 reshape.217
  86.1 3.2 %all-to-all-start.1 = ((bf16[4,2,256]{2,1,0:T(2,128)(2,1)}), bf16[4,2,256]{2,1,0:T(2,128)(2,1)S(1)}, u32[]{:S(2)}, u32[]{:S(2)}) async-start(bf16[4,2,256]{2,1,0:T(2,128)(2,1)} %reshape.217), calls=%async_computation.1 | async-start | bytes 8192 | tf_op jit(solution)/shard_map/all_to_all | solution.py:115
  90.2 4.7 %all-to-all-done.1 = bf16[4,2,256]{2,1,0:T(2,128)(2,1)S(1)} async-done(((bf16[4,2,256]{2,1,0:T(2,128)(2,1)}), bf16[4,2,256]{2,1,0:T(2,128)(2,1)S(1)}, u32[]{:S(2)}, u32[]{:S(2)}) %all-to-all-start.1) | async-done | bytes 4128 | tf_op jit(solution)/shard_map/all_to_all | solution.py:115
  95.2 1.9 %fusion.33 = f32[64,1,32]{2,1,0:T(1,128)S(1)} fusion(f32[64,128,1]{1,2,0:T(1,128)S(1)} %bitcast.110, f32[1,64,32,128]{3,2,1,0:T(8,128)S(1)} %copy-done.1, f32[64,128]{1,0:T(8,128)S(1)} %broadcast_bitcast_fusion, f32[64,32]{1,0:T(8,128)S(1)} %copy.28, f32[64]{0:T(128)S(1)} %get-tuple-element.7), kind=kOutput, calls=%fused_computation.28 | convolution fusion | flops 3932160 | bytes 1130752 | tf_op jit(solution)/shard_map/shpn,shn->shp/dot_general | solution.py:67
  97.2 13.1 %all-gather.1 = bf16[4,64,32]{1,2,0:T(8,128)(2,1)S(1)} all-gather(bf16[1,64,32]{1,2,0:T(8,128)(2,1)S(1)} %fusion.64), channel_id=2, replica_groups=mesh['dp'=4,'kv'=4,'tp'=2] {'kv'}, dimensions={0}, use_global_device_ids=true | all-gather | bytes 20480 | tf_op jit(solution)/shard_map/all_gather | solution.py:136
  110.5 2.0 %convolution_bitcast_fusion = f32[4,512]{1,0:T(4,128)S(1)} fusion(bf16[4,64,32]{2,0,1:T(4,128)(2,1)S(1)} %copy.35, bf16[64,32,512]{2,1,0:T(8,128)(2,1)} %param.35), kind=kOutput, calls=%fused_computation.25 | convolution fusion | flops 8388608 | bytes 2121728 | tf_op jit(solution)/shard_map/dot_general | solution.py:137
  112.5 2.5 %psum.37 = f32[4,512]{1,0:T(4,128)S(1)} all-reduce(f32[4,512]{1,0:T(4,128)S(1)} %convolution_bitcast_fusion), channel_id=1, replica_groups=mesh['dp'=4,'kv'=4,'tp'=2] {'tp'}, use_global_device_ids=true, to_apply=%region_8.9 | all-reduce | flops 2048 | bytes 16384 | tf_op jit(solution)/shard_map/psum | solution.py:186
  115.0 13.2 %all_gather.15 = bf16[4,2048]{1,0:T(4,128)(2,1)S(1)} all-gather(bf16[4,512]{1,0:T(4,128)(2,1)S(1)} %add_convert_fusion), channel_id=1, replica_groups=mesh['dp'=4,'kv'=4,'tp'=2] {'kv'}, dimensions={1}, use_global_device_ids=true | all-gather | bytes 20480 | tf_op jit(solution)/shard_map/all_gather | solution.py:187
  128.3 2.7 %fusion.4 = f32[4,704]{1,0:T(4,128)S(1)} fusion(bf16[2,2048,704]{1,2,0:T(8,128)(2,1)} %param.20, f32[2048]{0:T(1024)S(1)} %bitcast.111, f32[4]{0:T(128)S(1)} %add_rsqrt_fusion, bf16[4,2048]{1,0:T(4,128)(2,1)S(1)} %all_gather.15), kind=kOutput, calls=%fused_computation.4 | convolution fusion | flops 11567104 | bytes 2919440 | tf_op jit(solution)/shard_map/dot_general | solution.py:18
  131.0 4.4 %fusion = f32[4,2048]{1,0:T(4,128)S(1)} fusion(bf16[2,704,2048]{2,1,0:T(8,128)(2,1)} %param.22, bf16[2,2048,704]{1,2,0:T(8,128)(2,1)} %param.21, f32[4,704]{1,0:T(4,128)S(1)} %fusion.4, f32[2048]{0:T(1024)S(1)} %bitcast.112, f32[4]{0:T(128)S(1)} %add_rsqrt_fusion, bf16[4,2048]{1,0:T(4,128)(2,1)S(1)} %all_gather.15), kind=kOutput, calls=%fused_computation | convolution fusion | flops 23118336 | bytes 5835792 | tf_op jit(solution)/shard_map/dot_general | solution.py:21
  135.4 16.2 %psum.38 = f32[4,2048]{1,0:T(4,128)S(1)} all-reduce(f32[4,2048]{1,0:T(4,128)S(1)} %fusion), channel_id=1, replica_groups=mesh['dp'=4,'kv'=4,'tp'=2] {'kv'}, use_global_device_ids=true, to_apply=%region_10.11 | all-reduce | flops 8192 | bytes 65536 | tf_op jit(solution)/shard_map/psum | solution.py:29
  151.6 3.4 %psum.39 = f32[4,2048]{1,0:T(4,128)S(1)} all-reduce(f32[4,2048]{1,0:T(4,128)S(1)} %psum.38), channel_id=1, replica_groups=mesh['dp'=4,'kv'=4,'tp'=2] {'tp'}, use_global_device_ids=true, to_apply=%region_11.12 | all-reduce | flops 8192 | bytes 65536 | tf_op jit(solution)/shard_map/psum | solution.py:29
  (56 shorter events, 4.1 us)
Async XLA Ops:
  0.0 55.1 %copy-start = (bf16[2048,16,32]{0,2,1:T(8,128)(2,1)S(1)}, bf16[2048,16,32]{0,2,1:T(8,128)(2,1)}, u32[]{:S(2)}) copy-start(bf16[2048,16,32]{0,2,1:T(8,128)(2,1)} %param.23) | copy-start | bytes 6291460
  34.8 27.2 %copy-start.2 = (bf16[512,64]{0,1:T(8,128)(2,1)S(1)}, bf16[512,64]{0,1:T(8,128)(2,1)}, u32[]{:S(2)}) copy-start(bf16[512,64]{0,1:T(8,128)(2,1)} %param.26) | copy-start | bytes 196612
  55.1 9.1 %copy-start.10 = (u32[32]{0:T(128)S(1)}, u32[32]{0:T(128)}, u32[]{:S(2)}) copy-start(u32[32]{0:T(128)} %constant.45) | copy-start | bytes 388
  55.1 30.2 %copy-start.5 = (bf16[4,2,8,128]{3,2,1,0:T(8,128)(2,1)S(1)}, bf16[4,2,8,128]{3,2,1,0:T(8,128)(2,1)}, u32[]{:S(2)}) copy-start(bf16[4,2,8,128]{3,2,1,0:T(8,128)(2,1)} %param.31) | copy-start | bytes 49156
  55.1 30.2 %copy-start.6 = (bf16[1,3,2,8,128]{4,3,2,1,0:T(8,128)(2,1)S(1)}, bf16[1,3,2,8,128]{4,3,2,1,0:T(8,128)(2,1)}, u32[]{:S(2)}) copy-start(bf16[1,3,2,8,128]{4,3,2,1,0:T(8,128)(2,1)} %param.33) | copy-start | bytes 36868
  55.1 34.2 %copy-start.8 = (f32[64]{0:T(128)S(1)}, f32[64]{0:T(128)}, u32[]{:S(2)}) copy-start(f32[64]{0:T(128)} %param.28) | copy-start | bytes 772
  55.1 34.2 %copy-start.9 = (f32[64]{0:T(128)S(1)}, f32[64]{0:T(128)}, u32[]{:S(2)}) copy-start(f32[64]{0:T(128)} %param.27) | copy-start | bytes 772
  55.8 39.3 %copy-start.3 = (bf16[4,64,32]{1,2,0:T(8,128)(2,1)S(1)}, bf16[4,64,32]{1,2,0:T(8,128)(2,1)}, u32[]{:S(2)}) copy-start(bf16[4,64,32]{1,2,0:T(8,128)(2,1)} %param.30) | copy-start | bytes 49156
  55.8 39.3 %copy-start.4 = (bf16[1,3,64,32]{2,3,1,0:T(8,128)(2,1)S(1)}, bf16[1,3,64,32]{2,3,1,0:T(8,128)(2,1)}, u32[]{:S(2)}) copy-start(bf16[1,3,64,32]{2,3,1,0:T(8,128)(2,1)} %param.32) | copy-start | bytes 36868
  55.8 39.4 %copy-start.1 = (f32[1,64,32,128]{3,2,1,0:T(8,128)S(1)}, f32[1,64,32,128]{3,2,1,0:T(8,128)}, u32[]{:S(2)}) copy-start(f32[1,64,32,128]{3,2,1,0:T(8,128)} %param.34) | copy-start | bytes 3145732
  56.6 29.5 %all-to-all-start = ((bf16[4,2,256]{2,1,0:T(2,128)(2,1)}), bf16[4,2,256]{2,1,0:T(2,128)(2,1)S(1)}, u32[]{:S(2)}, u32[]{:S(2)}) async-start(bf16[4,2,256]{2,1,0:T(2,128)(2,1)} %reshape.219), calls=%async_computation | async-start | bytes 8192 | tf_op jit(solution)/shard_map/all_to_all | solution.py:114
  59.8 37.4 %copy-start.7 = (f32[64]{0:T(128)S(1)}, f32[64]{0:T(128)}, u32[]{:S(2)}) copy-start(f32[64]{0:T(128)} %param.29) | copy-start | bytes 772
  86.1 8.8 %all-to-all-start.1 = ((bf16[4,2,256]{2,1,0:T(2,128)(2,1)}), bf16[4,2,256]{2,1,0:T(2,128)(2,1)S(1)}, u32[]{:S(2)}, u32[]{:S(2)}) async-start(bf16[4,2,256]{2,1,0:T(2,128)(2,1)} %reshape.217), calls=%async_computation.1 | async-start | bytes 8192 | tf_op jit(solution)/shard_map/all_to_all | solution.py:115
